TPU v7x, 32 devices: a whole 2x2x4 slice. The times are simulated.
32 devices in a mesh: grp: 2 (over y), fs: 4 (over z), tp: 4 (over x, core).
Axes of the slice: x: 2, y: 2, z: 4, core: 2. Of those that a mesh axis runs over, the one named last changes fastest.
Arguments:
- tokens: bfloat16 [4096, 2048], P(('grp', 'fs', 'tp')), parts along dimension 0, may hold values from -12 to 12
- norm_gain: float32 [2048], replicated, may hold values from 0.1 to 1.9
- w_in: bfloat16 [2048, 8192], P('fs', 'tp'), may hold values from -0.125 to 0.125
- w_out: bfloat16 [8192, 2048], P('tp', 'fs'), may hold values from -0.0625 to 0.0625
Outputs:
- mixed: bfloat16 [4096, 2048], P(('grp', 'fs', 'tp')), parts along dimension 0
There are 2 independent parts, one for each index of `grp`. A program takes and returns all parts, laid end to end along the dimension named above; an argument that names none is the same for every part. Nothing has to cross between parts.
All inputs are finite; a program needn't handle non-finite values.
Results may differ from a plain program's by a relative error of at most 0.012.
Values may be sent and summed in bfloat16 or wider, within the bound.
A program may use at most 64 MiB of HBM per device.

v0:
```python
import functools

import jax
import jax.numpy as jnp
from jax import lax
from jax.experimental import pallas as pl
from jax.experimental.pallas import tpu as pltpu
from jax.sharding import PartitionSpec as P

EPS = 1e-06
MESH = pl.DeviceIdType.MESH
CORES = 2
PLANES = 2


def remote(src, dst, send, recv, device):
    pltpu.make_async_remote_copy(
        src_ref=src, dst_ref=dst, send_sem=send, recv_sem=recv, device_id=device, device_id_type=MESH
    ).start()


def done(ref, sem):
    pltpu.make_async_copy(ref, ref, sem).wait()


def kernel(
    Y, n, X, parts, x_ref, g_ref, wi_ref, wo_ref, o_ref,
    norm, wi, wo, hid, crecv, precv, zsend, zrecv, acc,
    tok_send, tok_recv, wi_send, wi_recv, wo_send, wo_recv,
    c_send, c_recv, p_send, p_recv, z_send, z_recv,
):
    y, i, j = lax.axis_index("grp"), lax.axis_index("fs"), lax.axis_index("tp")
    x, core, zp = j // CORES, j % CORES, i % PLANES
    chips = Y * X
    chip = y * X + x
    B, D = x_ref.shape
    HU = wi.shape[1]
    Dr, Dc = wi_ref.shape[0], wo_ref.shape[1]
    W = Dc // parts
    NC = n * parts
    R = norm.shape[0]
    half = R // CORES
    pair_rows = PLANES * B

    partner = (y, i, x * CORES + 1 - core)
    zpair = (y, i + 1 - 2 * zp, j)

    def at_chip(k):
        return (k // X, i, (k % X) * CORES + core)

    def other_chip(o):
        return lax.rem(chip + o, chips)

    direction = jnp.where(i < n // 2, 1, -1)

    barrier = pltpu.get_barrier_semaphore()
    for k in range(1, n):
        pl.semaphore_signal(barrier, inc=1, device_id=(y, lax.rem(i + k, n), j), device_id_type=MESH)
    pl.semaphore_signal(barrier, inc=1, device_id=partner, device_id_type=MESH)
    for o in range(1, chips):
        pl.semaphore_signal(barrier, inc=1, device_id=at_chip(other_chip(o)), device_id_type=MESH)

    def block(c, k, z):
        return (c * chips + k) * PLANES + z

    def rows_of(b):
        return pl.ds(pl.multiple_of(b * B, B), B)

    mine = block(core, chip, zp)

    @pl.loop(0, B // 16)
    def _(r):
        rows = pl.ds(pl.multiple_of(r * 16, 16), 16)
        xf = x_ref[rows, :].astype(jnp.float32)
        scale = lax.rsqrt(jnp.mean(xf * xf, axis=-1, keepdims=True) + EPS)
        out_rows = pl.ds(pl.multiple_of(mine * B + r * 16, 16), 16)
        norm[out_rows, :] = (xf * scale * g_ref[...]).astype(jnp.bfloat16)

    pl.semaphore_wait(barrier, (n - 1) + 1 + (chips - 1))

    count = [0]

    def send_block(b, device):
        ref = norm.at[rows_of(b), :]
        remote(ref, ref, tok_send.at[count[0]], tok_recv.at[b], device)
        count[0] += 1

    send_block(mine, zpair)
    for o in range(1, chips):
        send_block(mine, at_chip(other_chip(o)))
    send_block(mine, partner)

    def in_cols(d):
        return pl.ds(pl.multiple_of(((d % PLANES) * Y + y) * HU, HU), HU)

    def in_rows(s):
        return pl.ds(pl.multiple_of(s * Dr, Dr), Dr)

    def out_cols(cid):
        return pl.ds(pl.multiple_of(cid * W, W), W)

    near = i + 1 - 2 * zp

    def to_planes(send):
        for k in range(1, n):
            d = lax.rem(i + n + direction * k, n)
            pl.when(d != near)(functools.partial(send, d))
        send(near)

    def send_in(d):
        remote(wi_ref.at[:, in_cols(d)], wi.at[in_rows(i), :], wi_send.at[d], wi_recv.at[i], (y, d, j))

    def send_out(h, d):
        cid = i * parts + h
        remote(
            wo_ref.at[in_cols(d), pl.ds(h * W, W)], wo.at[:, out_cols(cid)],
            wo_send.at[d * parts + h], wo_recv.at[cid], (y, d, j),
        )

    to_planes(send_in)
    pltpu.make_async_copy(wi_ref.at[:, in_cols(i)], wi.at[in_rows(i), :], wi_recv.at[i]).start()
    for h in range(parts):
        to_planes(functools.partial(send_out, h))
        cid = i * parts + h
        pltpu.make_async_copy(
            wo_ref.at[in_cols(i), pl.ds(h * W, W)], wo.at[:, out_cols(cid)], wo_recv.at[cid]
        ).start()

    def arrived(b):
        done(norm.at[rows_of(b), :], tok_recv.at[b])

    paired = block(core, chip, 1 - zp)
    arrived(paired)
    for o in range(1, chips):
        send_block(paired, at_chip(other_chip(o)))
    send_block(paired, partner)
    for z in (zp, 1 - zp):
        for o in range(1, chips):
            b = block(core, other_chip(chips - o), z)
            arrived(b)
            send_block(b, partner)
    for o in range(chips):
        for z in range(PLANES):
            arrived(block(1 - core, other_chip(o), z))

    for s in range(n):
        done(wi.at[in_rows(s), :], wi_recv.at[s])

    TR = min(256, half)

    @pl.loop(0, R // TR)
    def _(r):
        rows = pl.ds(pl.multiple_of(r * TR, TR), TR)
        pre = jnp.dot(norm[rows, :], wi[...], preferred_element_type=jnp.float32)
        hid[rows, :] = jnp.square(jnp.maximum(pre, 0.0)).astype(jnp.bfloat16)

    for q in range(count[0]):
        done(norm.at[rows_of(0), :], tok_send.at[q])

    kept, given = core * half, (1 - core) * half

    def chunk(t):
        s = lax.rem(i + n + direction * (t % n), n)
        return s * parts + t // n

    def multiply(first, cols):
        @pl.loop(0, half // TR)
        def _(r):
            rows = pl.ds(pl.multiple_of(first + r * TR, TR), TR)
            norm[rows, cols] = jnp.dot(
                hid[rows, :], wo[:, cols], preferred_element_type=jnp.float32
            ).astype(jnp.bfloat16)

    def chip_rows(base, k):
        return pl.ds(pl.multiple_of(base + k * pair_rows, pair_rows), pair_rows)

    def fold(k, cols):
        rows = chip_rows(kept, k)
        norm[rows, cols] = (
            norm[rows, cols].astype(jnp.float32) + crecv[chip_rows(0, k), cols].astype(jnp.float32)
        ).astype(jnp.bfloat16)

    @pl.loop(0, NC + 2)
    def _(t):
        @pl.when(t < NC)
        def _():
            cid = chunk(t)
            cols = out_cols(cid)
            done(wo.at[:, cols], wo_recv.at[cid])
            multiply(given, cols)
            remote(
                norm.at[pl.ds(pl.multiple_of(given, half), half), cols], crecv.at[:, cols],
                c_send.at[cid], c_recv.at[cid], partner,
            )
            multiply(kept, cols)
            done(crecv.at[:, cols], c_recv.at[cid])
            for o in range(1, chips):
                k = other_chip(o)
                fold(k, cols)
                remote(
                    norm.at[chip_rows(kept, k), cols], precv.at[chip, :, cols],
                    p_send.at[cid * chips + k], p_recv.at[cid * chips + chip], at_chip(k),
                )
            fold(chip, cols)

        @pl.when(t >= 2)
        def _():
            cid = chunk(t - 2)
            cols = out_cols(cid)
            for o in range(1, chips):
                k = other_chip(o)
                done(precv.at[k, :, cols], p_recv.at[cid * chips + k])

            def total(z):
                inner = pl.ds(pl.multiple_of(z * B, B), B)
                first = kept + chip * pair_rows + z * B
                value = norm[pl.ds(pl.multiple_of(first, B), B), cols].astype(jnp.float32)
                for o in range(1, chips):
                    value += precv[other_chip(o), inner, cols].astype(jnp.float32)
                return value

            zsend[:, cols] = total(1 - zp).astype(jnp.bfloat16)
            remote(zsend.at[:, cols], zrecv.at[:, cols], z_send.at[cid], z_recv.at[cid], zpair)
            acc[:, cols] = total(zp)

    @pl.loop(0, NC)
    def _(t):
        cid = chunk(t)
        cols = out_cols(cid)
        done(zrecv.at[:, cols], z_recv.at[cid])
        total = acc[:, cols] + zrecv[:, cols].astype(jnp.float32)
        o_ref[:, cols] = (x_ref[:, cols].astype(jnp.float32) + total).astype(jnp.bfloat16)

    for k in range(1, n):
        d = lax.rem(i + k, n)
        done(wi.at[in_rows(0), :], wi_send.at[d])
        for h in range(parts):
            done(wo.at[:, out_cols(0)], wo_send.at[d * parts + h])

    @pl.loop(0, NC)
    def _(cid):
        cols = out_cols(cid)
        done(crecv.at[:, cols], c_send.at[cid])
        done(zsend.at[:, cols], z_send.at[cid])
        for o in range(1, chips):
            k = other_chip(o)
            done(precv.at[k, :, cols], p_send.at[cid * chips + k])


def solution(mesh):
    Y, n, T = mesh.shape["grp"], mesh.shape["fs"], mesh.shape["tp"]
    X = T // CORES
    chips = Y * X

    def local(tokens, norm_gain, w_in, w_out):
        B, D = tokens.shape
        HU = w_in.shape[1] // (PLANES * Y)
        Dc = w_out.shape[1]
        parts = Dc // 128
        NC = n * parts
        R = CORES * chips * PLANES * B
        sends = 1 + chips + chips + PLANES * (chips - 1)
        bf16 = jnp.bfloat16
        dma = pltpu.SemaphoreType.DMA
        vmem = pl.BlockSpec(memory_space=pltpu.VMEM)
        hbm = pl.BlockSpec(memory_space=pl.ANY)
        return pl.pallas_call(
            functools.partial(kernel, Y, n, X, parts),
            out_shape=jax.ShapeDtypeStruct((B, D), bf16),
            in_specs=[vmem, vmem, hbm, hbm],
            out_specs=vmem,
            scratch_shapes=[
                pltpu.VMEM((R, D), bf16),
                pltpu.VMEM((D, HU), bf16),
                pltpu.VMEM((HU, D), bf16),
                pltpu.VMEM((R, HU), bf16),
                pltpu.VMEM((R // CORES, D), bf16),
                pltpu.VMEM((chips, PLANES * B, D), bf16),
                pltpu.VMEM((B, D), bf16),
                pltpu.VMEM((B, D), bf16),
                pltpu.VMEM((B, D), jnp.float32),
                dma((sends,)), dma((CORES * chips * PLANES,)),
                dma((n,)), dma((n,)),
                dma((NC,)), dma((NC,)),
                dma((NC,)), dma((NC,)),
                dma((NC * chips,)), dma((NC * chips,)),
                dma((NC,)), dma((NC,)),
            ],
            compiler_params=pltpu.CompilerParams(
                collective_id=0, has_side_effects=True, vmem_limit_bytes=60 * 1024 * 1024
            ),
        )(tokens, norm_gain.reshape(1, D), w_in, w_out)

    in_specs = (P(("grp", "fs", "tp"), None), P(), P("fs", "tp"), P("tp", "fs"))
    out_specs = P(("grp", "fs", "tp"), None)
    return jax.shard_map(local, mesh=mesh, in_specs=in_specs, out_specs=out_specs, check_vma=False)
```

profile of v0, /device:TPU:0, one launch (start us, length us, event | category | flops | bytes accessed | tf_op | source)
XLA Modules:
  0.0 128.0 jit_solution(6057753380366257568)
XLA Ops:
  0.0 126.1 %shard_map.46 = bf16[128,2048]{1,0:T(8,128)(2,1)} custom-call(bf16[128,2048]{1,0:T(8,128)(2,1)} %x_ref.1, f32[1,2048]{1,0:T(1,128)} %bitcast.1, bf16[512,2048]{1,0:T(8,128)(2,1)} %wi_ref.1, bf16[2048,512]{1,0:T(8,128)(2,1)} %wo_ref.1), custom_call_target="tpu_custom_call" | custom-call | tf_op jit(solution)/shard_map/pallas_call | solution.py:267
  126.1 1.9 %copy.6 = bf16[128,2048]{1,0:T(8,128)(2,1)} copy(bf16[128,2048]{1,0:T(8,128)(2,1)} %shard_map.46) | data formatting | bytes 1048576
where the time goes:
time: 128 us
  Pallas kernels  126 us (98%)
  local copies, waits for them, and re-layouts  1.88 us (1%)
    pallas_call x1, Pallas kernels, local(): pl.pallas_call(functools.partial(kernel, Y, n, X, parts), out_shape=jax.S...  126 us

commit v1 on v0

v1 whole, which is shorter than its diff:
```python
import functools

import jax
import jax.numpy as jnp
from jax import lax
from jax.experimental import pallas as pl
from jax.experimental.pallas import tpu as pltpu
from jax.sharding import PartitionSpec as P

EPS = 1e-06
MESH = pl.DeviceIdType.MESH
CORES = 2
PLANES = 2
LAG_1, LAG_2, LAG_3, LAG_4 = 1, 3, 6, 8


def remote(src, dst, send, recv, device):
    pltpu.make_async_remote_copy(
        src_ref=src, dst_ref=dst, send_sem=send, recv_sem=recv, device_id=device, device_id_type=MESH
    ).start()


def done(ref, sem):
    pltpu.make_async_copy(ref, ref, sem).wait()


def f32(value):
    return value.astype(jnp.float32)


def kernel(
    Y, n, X, parts, x_hbm, g_ref, wi_ref, wo_ref, o_hbm,
    norm, wi, wo, hid, crecv, yl, xf, xl, yf, own_l, own_f, zsend, zrecv, x_ref, out,
    x_sem, o_sem, tok_send, tok_recv, wi_send, wi_recv, wo_send, wo_recv, wi_fwd, wo_fwd,
    c_send, c_recv, yl_send, yl_recv, xf_send, xf_recv, xl_send, xl_recv, yf_send, yf_recv, z_send, z_recv,
):
    y, i, j = lax.axis_index("grp"), lax.axis_index("fs"), lax.axis_index("tp")
    x, core, zp = j // CORES, j % CORES, i % PLANES
    chips = Y * X
    B, D = x_ref.shape
    HU = wi.shape[1]
    Dr, Dc = wi_ref.shape[0], wo_ref.shape[1]
    W = Dc // parts
    NC = n * parts
    R = norm.shape[0]
    half = R // CORES
    region = chips * B

    partner = (y, i, x * CORES + 1 - core)
    near = i + 1 - 2 * zp
    zpair = (y, near, j)

    def plane(d):
        return (y, d, j)

    def at(yy, xx):
        return (yy, i, xx * CORES + core)

    def turn(v, o, size):
        return lax.rem(v + o, size)

    others = [(oy, ox) for oy in range(Y) for ox in range(X) if oy or ox]

    def has(d):
        return (d >= 0) & (d < n)

    HOPS = (1, 2, -1, -2)

    load_x = pltpu.make_async_copy(x_hbm, x_ref, x_sem)
    load_x.start()

    barrier = pltpu.get_barrier_semaphore()
    peers = len(others) + 1
    for step in HOPS:
        there = has(i + step)
        peers += there.astype(jnp.int32)

        @pl.when(there)
        def _():
            pl.semaphore_signal(barrier, inc=1, device_id=plane(i + step), device_id_type=MESH)

    pl.semaphore_signal(barrier, inc=1, device_id=partner, device_id_type=MESH)
    for oy, ox in others:
        pl.semaphore_signal(
            barrier, inc=1, device_id=at(turn(y, oy, Y), turn(x, ox, X)), device_id_type=MESH
        )

    def block_l(c, yy, xx):
        return c * PLANES * chips + yy * X + xx

    def block_f(c, yy, xx):
        return (c * PLANES + 1) * chips + xx * Y + yy

    def rows_at(first, size):
        return pl.ds(pl.multiple_of(first, B), size)

    def rows_of(b):
        return rows_at(b * B, B)

    mine, paired = block_l(core, y, x), block_f(core, y, x)

    def in_cols(d):
        return pl.ds(pl.multiple_of(((d % PLANES) * Y + y) * HU, HU), HU)

    def in_rows(s):
        return pl.ds(pl.multiple_of(s * Dr, Dr), Dr)

    def out_cols(cid):
        return pl.ds(pl.multiple_of(cid * W, W), W)

    pltpu.make_async_copy(wi_ref.at[:, in_cols(i)], wi.at[in_rows(i), :], wi_recv.at[i]).start()
    for h in range(parts):
        cid = i * parts + h
        pltpu.make_async_copy(
            wo_ref.at[in_cols(i), pl.ds(h * W, W)], wo.at[:, out_cols(cid)], wo_recv.at[cid]
        ).start()

    load_x.wait()

    @pl.loop(0, B // 16)
    def _(r):
        rows = pl.ds(pl.multiple_of(r * 16, 16), 16)
        v = f32(x_ref[rows, :])
        scale = lax.rsqrt(jnp.mean(v * v, axis=-1, keepdims=True) + EPS)
        out_rows = pl.ds(pl.multiple_of(mine * B + r * 16, 16), 16)
        norm[out_rows, :] = (v * scale * g_ref[...]).astype(jnp.bfloat16)

    pl.semaphore_wait(barrier, peers)

    def send_in(step):
        d = i + step
        k = HOPS.index(step)

        @pl.when(has(d))
        def _():
            remote(wi_ref.at[:, in_cols(d)], wi.at[in_rows(i), :], wi_send.at[k], wi_recv.at[i], plane(d))

    def send_out(h, step):
        d = i + step
        k = HOPS.index(step)

        @pl.when(has(d))
        def _():
            cid = i * parts + h
            remote(
                wo_ref.at[in_cols(d), pl.ds(pl.multiple_of(h * W, W), W)], wo.at[:, out_cols(cid)],
                wo_send.at[h, k], wo_recv.at[cid], plane(d),
            )

    def both_ways(send):
        for sign in (1, -1):
            relayed = has(i + 3 * sign)

            @pl.when(relayed)
            def _():
                send(sign)
                send(2 * sign)

            @pl.when(jnp.logical_not(relayed))
            def _():
                send(2 * sign)
                send(sign)

    def onward(s):
        return jnp.where(s < i, i + 2, i - 2)

    def relays(s):
        return (s != i) & has(onward(s))

    def relay_in(s):
        @pl.when(relays(s))
        def _():
            ref = wi.at[in_rows(s), :]
            remote(ref, ref, wi_fwd.at[s], wi_recv.at[s], plane(onward(s)))

    def relay_out(cid):
        s = cid // parts

        @pl.when(relays(s))
        def _():
            ref = wo.at[:, out_cols(cid)]
            remote(ref, ref, wo_fwd.at[cid], wo_recv.at[cid], plane(onward(s)))

    count = [0]

    def send_block(b, device, into=None):
        into = b if into is None else into
        remote(
            norm.at[rows_of(b), :], norm.at[rows_of(into), :],
            tok_send.at[count[0]], tok_recv.at[into], device,
        )
        count[0] += 1

    send_block(mine, zpair, paired)
    both_ways(send_in)
    for oy, ox in others:
        send_block(mine, at(turn(y, oy, Y), turn(x, ox, X)))
    send_block(mine, partner)

    def arrived(b):
        done(norm.at[rows_of(b), :], tok_recv.at[b])

    arrived(paired)
    for oy, ox in others:
        send_block(paired, at(turn(y, oy, Y), turn(x, ox, X)))
    send_block(paired, partner)

    def in_arrived(s):
        done(wi.at[in_rows(s), :], wi_recv.at[s])
        relay_in(s)

    def source(k):
        if k == 0:
            return i
        if k == 1:
            return near
        pair = lax.rem(i // PLANES + k // PLANES, n // PLANES)
        e = k % PLANES
        return jnp.where(pair > i // PLANES, pair * PLANES + e, pair * PLANES + PLANES - 1 - e)

    inner = relays(near)

    @pl.when(jnp.logical_not(inner))
    def _():
        for h in range(parts):
            both_ways(functools.partial(send_out, h))

    in_arrived(source(1))

    @pl.when(inner)
    def _():
        both_ways(functools.partial(send_out, 0))

    def near_out(h):
        cid = near * parts + h
        done(wo.at[:, out_cols(cid)], wo_recv.at[cid])

        @pl.when(inner)
        def _():
            relay_out(cid)
            pl.when(h + 1 < parts)(lambda: both_ways(functools.partial(send_out, h + 1)))

    for block in (block_l, block_f):
        for oy, ox in others:
            b = block(core, turn(y, Y - oy, Y), turn(x, X - ox, X))
            arrived(b)
            send_block(b, partner)
    for yy in range(Y):
        for xx in range(X):
            arrived(block_l(1 - core, yy, xx))
            arrived(block_f(1 - core, yy, xx))

    in_arrived(source(0))
    for k in range(2, n):
        in_arrived(source(k))

    near_out(0)

    TR = min(512, half)

    @pl.loop(0, R // TR)
    def _(r):
        rows = pl.ds(pl.multiple_of(r * TR, TR), TR)
        pre = jnp.dot(norm[rows, :], wi[...], preferred_element_type=jnp.float32)
        hid[rows, :] = jnp.square(jnp.maximum(pre, 0.0)).astype(jnp.bfloat16)

    for q in range(count[0]):
        done(norm.at[rows_of(0), :], tok_send.at[q])

    kept, given = core * half, (1 - core) * half

    def chunk(t):
        k, h = t % n, t // n
        pair = lax.rem(i // PLANES + k // PLANES, n // PLANES)
        e = k % PLANES
        far = jnp.where(pair > i // PLANES, pair * PLANES + e, pair * PLANES + PLANES - 1 - e)
        s = jnp.where(k == 0, near, jnp.where(k == 1, i, far))
        return s * parts + h

    TM = min(1024, half)

    def multiply(first, cols):
        for r in range(half // TM):
            rows = pl.ds(pl.multiple_of(first + r * TM, TM), TM)
            norm[rows, cols] = jnp.dot(
                hid[rows, :], wo[:, cols], preferred_element_type=jnp.float32
            ).astype(jnp.bfloat16)

    def fold(first, size, cols):
        rows = rows_at(kept + first, size)
        norm[rows, cols] = (f32(norm[rows, cols]) + f32(crecv[rows_at(first, size), cols])).astype(jnp.bfloat16)

    SL, SF = X * B, Y * B

    def part_sum(first, cols, landed, others_of, inside):
        v = f32(norm[rows_at(kept + first, B), cols]) + f32(crecv[rows_at(first, B), cols])
        for o in others_of:
            v += f32(landed[o, rows_at(inside, B), cols])
        return v

    def product(t):
        cid = chunk(t)
        cols = out_cols(cid)
        k, h = t % n, t // n

        @pl.when(k > 0)
        def _():
            done(wo.at[:, cols], wo_recv.at[cid])
            relay_out(cid)

        pl.when((k == 1) & (h + 1 < parts))(lambda: near_out(h + 1))

        multiply(given, cols)
        remote(
            norm.at[rows_at(given, half), cols], crecv.at[:, cols], c_send, c_recv.at[cid], partner
        )
        multiply(kept, cols)

    def first_stage(t):
        cid = chunk(t)
        cols = out_cols(cid)
        done(crecv.at[:, cols], c_recv.at[cid])
        for o in range(1, X):
            xx = turn(x, o, X)
            fold(region + xx * SF, SF, cols)
            remote(
                norm.at[rows_at(kept + region + xx * SF, SF), cols], xf.at[x, :, cols],
                xf_send, xf_recv.at[cid * X + x], at(y, xx),
            )
        for o in range(1, Y):
            yy = turn(y, o, Y)
            fold(yy * SL, SL, cols)
            remote(
                norm.at[rows_at(kept + yy * SL, SL), cols], yl.at[y, :, cols],
                yl_send, yl_recv.at[cid * Y + y], at(yy, x),
            )

    def second_stage(t):
        cid = chunk(t)
        cols = out_cols(cid)
        xs = [turn(x, o, X) for o in range(1, X)]
        ys = [turn(y, o, Y) for o in range(1, Y)]
        for xx in xs:
            done(xf.at[xx, :, cols], xf_recv.at[cid * X + xx])
        for yy in ys:
            first = region + x * SF + yy * B
            norm[rows_at(kept + first, B), cols] = part_sum(first, cols, xf, xs, yy * B).astype(jnp.bfloat16)
            remote(
                norm.at[rows_at(kept + first, B), cols], yf.at[y, :, cols],
                yf_send, yf_recv.at[cid * Y + y], at(yy, x),
            )
        for yy in ys:
            done(yl.at[yy, :, cols], yl_recv.at[cid * Y + yy])
        for xx in xs:
            first = y * SL + xx * B
            norm[rows_at(kept + first, B), cols] = part_sum(first, cols, yl, ys, xx * B).astype(jnp.bfloat16)
            remote(
                norm.at[rows_at(kept + first, B), cols], xl.at[x, :, cols],
                xl_send, xl_recv.at[cid * X + x], at(y, xx),
            )
        own_f[:, cols] = part_sum(region + x * SF + y * B, cols, xf, xs, y * B)
        own_l[:, cols] = part_sum(y * SL + x * B, cols, yl, ys, x * B)

    def third_stage(t):
        cid = chunk(t)
        cols = out_cols(cid)
        v = own_f[:, cols]
        for o in range(1, Y):
            yy = turn(y, o, Y)
            done(yf.at[yy, :, cols], yf_recv.at[cid * Y + yy])
            v += f32(yf[yy, :, cols])
        zsend[:, cols] = v.astype(jnp.bfloat16)
        remote(zsend.at[:, cols], zrecv.at[:, cols], z_send, z_recv.at[cid], zpair)
        v = own_l[:, cols]
        for o in range(1, X):
            xx = turn(x, o, X)
            done(xl.at[xx, :, cols], xl_recv.at[cid * X + xx])
            v += f32(xl[xx, :, cols])
        own_l[:, cols] = v

    def finish(t):
        cid = chunk(t)
        cols = out_cols(cid)
        done(zrecv.at[:, cols], z_recv.at[cid])
        v = own_l[:, cols] + f32(zrecv[:, cols])
        out[:, cols] = (f32(x_ref[:, cols]) + v).astype(jnp.bfloat16)
        pltpu.make_async_copy(out.at[:, cols], o_hbm.at[:, cols], o_sem).start()

    stages = ((0, product), (LAG_1, first_stage), (LAG_2, second_stage), (LAG_3, third_stage), (LAG_4, finish))

    @pl.loop(0, NC + LAG_4)
    def _(t):
        for lag, stage in stages:
            pl.when((t >= lag) & (t < NC + lag))(functools.partial(stage, t - lag))

    for k, step in enumerate(HOPS):
        @pl.when(has(i + step))
        def _():
            done(wi.at[in_rows(0), :], wi_send.at[k])
            for h in range(parts):
                done(wo.at[:, out_cols(0)], wo_send.at[h, k])

    for s in range(n):
        @pl.when(relays(s))
        def _():
            done(wi.at[in_rows(0), :], wi_fwd.at[s])
            for h in range(parts):
                done(wo.at[:, out_cols(0)], wo_fwd.at[s * parts + h])

    done(crecv, c_send)
    if Y > 1:
        done(yl.at[pl.ds(0, Y - 1)], yl_send)
        done(yf.at[pl.ds(0, Y - 1)], yf_send)
    if X > 1:
        done(xf.at[pl.ds(0, X - 1)], xf_send)
        done(xl.at[pl.ds(0, X - 1)], xl_send)
    done(zsend, z_send)
    pltpu.make_async_copy(out, o_hbm, o_sem).wait()


def solution(mesh):
    Y, n, T = mesh.shape["grp"], mesh.shape["fs"], mesh.shape["tp"]
    X = T // CORES
    chips = Y * X

    def local(tokens, norm_gain, w_in, w_out):
        B, D = tokens.shape
        HU = w_in.shape[1] // (PLANES * Y)
        parts = w_out.shape[1] // 128
        NC = n * parts
        R = CORES * chips * PLANES * B
        sends = 1 + 2 * chips + PLANES * (chips - 1)
        bf16 = jnp.bfloat16
        dma = pltpu.SemaphoreType.DMA
        vmem = pl.BlockSpec(memory_space=pltpu.VMEM)
        hbm = pl.BlockSpec(memory_space=pl.ANY)
        return pl.pallas_call(
            functools.partial(kernel, Y, n, X, parts),
            out_shape=jax.ShapeDtypeStruct((B, D), bf16),
            in_specs=[hbm, vmem, hbm, hbm],
            out_specs=hbm,
            scratch_shapes=[
                pltpu.VMEM((R, D), bf16),
                pltpu.VMEM((D, HU), bf16),
                pltpu.VMEM((HU, D), bf16),
                pltpu.VMEM((R, HU), bf16),
                pltpu.VMEM((R // CORES, D), bf16),
                pltpu.VMEM((Y, X * B, D), bf16),
                pltpu.VMEM((X, Y * B, D), bf16),
                pltpu.VMEM((X, B, D), bf16),
                pltpu.VMEM((Y, B, D), bf16),
                pltpu.VMEM((B, D), jnp.float32),
                pltpu.VMEM((B, D), jnp.float32),
                pltpu.VMEM((B, D), bf16),
                pltpu.VMEM((B, D), bf16),
                pltpu.VMEM((B, D), bf16),
                pltpu.VMEM((B, D), bf16),
                dma, dma,
                dma((sends,)), dma((CORES * chips * PLANES,)),
                dma((4,)), dma((n,)),
                dma((parts, 4)), dma((NC,)),
                dma((n,)), dma((NC,)),
                dma, dma((NC,)),
                dma, dma((NC * Y,)),
                dma, dma((NC * X,)),
                dma, dma((NC * X,)),
                dma, dma((NC * Y,)),
                dma, dma((NC,)),
            ],
            compiler_params=pltpu.CompilerParams(
                collective_id=0, has_side_effects=True, vmem_limit_bytes=60 * 1024 * 1024
            ),
        )(tokens, norm_gain.reshape(1, D), w_in, w_out)

    in_specs = (P(("grp", "fs", "tp"), None), P(), P("fs", "tp"), P("tp", "fs"))
    out_specs = P(("grp", "fs", "tp"), None)
    return jax.shard_map(local, mesh=mesh, in_specs=in_specs, out_specs=out_specs, check_vma=False)
```

time: 128 us -> 122 us (0.953)
  Pallas kernels: 126 us -> 119 us
    pallas_call x1, Pallas kernels: 126 us -> 119 us  [local(): pl.pallas_call(functools.partial(kernel, Y, n, X, parts), out_shape=jax.S...]
where the time goes in v1:
time: 122 us; the launch traced here: 121 us
  Pallas kernels  119 us (98%)
  local copies, waits for them, and re-layouts  1.88 us (2%)
    pallas_call x1, Pallas kernels, local(): pl.pallas_call(functools.partial(kernel, Y, n, X, parts), out_shape=jax.S...  119 us

profile of v1, /device:TPU:0, one launch (start us, length us, event | category | flops | bytes accessed | tf_op | source)
XLA Modules:
  0.0 121.4 jit_solution(9916579235160953562)
XLA Ops:
  0.0 119.5 %shard_map.46 = bf16[128,2048]{1,0:T(8,128)(2,1)} custom-call(bf16[128,2048]{1,0:T(8,128)(2,1)} %x_hbm.1, f32[1,2048]{1,0:T(1,128)} %bitcast.1, bf16[512,2048]{1,0:T(8,128)(2,1)} %wi_ref.1, bf16[2048,512]{1,0:T(8,128)(2,1)} %wo_ref.1), custom_call_target="tpu_custom_call" | custom-call | tf_op jit(solution)/shard_map/pallas_call | solution.py:437
  119.5 1.9 %copy.6 = bf16[128,2048]{1,0:T(8,128)(2,1)} copy(bf16[128,2048]{1,0:T(8,128)(2,1)} %shard_map.46) | data formatting | bytes 1048576

commit v2 on v1

--- a/solution.py
+++ b/solution.py
@@ -11,7 +11,8 @@
 MESH = pl.DeviceIdType.MESH
 CORES = 2
 PLANES = 2
-LAG_1, LAG_2, LAG_3, LAG_4 = 1, 3, 6, 8
+FAR_STEP = 0.0
+LAG_1, LAG_2, LAG_3, LAG_4 = 1, 3, 5, 7
 
 
 def remote(src, dst, send, recv, device):
@@ -220,16 +221,28 @@
 
     inner = relays(near)
 
-    @pl.when(jnp.logical_not(inner))
+    def out_near(h):
+        for step in (1, -1):
+            pl.when(i + step == near)(functools.partial(send_out, h, step))
+
+    def out_far(h):
+        for step in (2, 1, -2, -1):
+            pl.when(i + step != near)(functools.partial(send_out, h, step))
+
+    def outer_out():
+        for h in range(parts):
+            out_near(h)
+        for h in range(parts):
+            out_far(h)
+
+    pl.when(jnp.logical_not(inner))(outer_out)
+    in_arrived(source(1))
+
+    @pl.when(inner)
     def _():
         for h in range(parts):
-            both_ways(functools.partial(send_out, h))
-
-    in_arrived(source(1))
-
-    @pl.when(inner)
-    def _():
-        both_ways(functools.partial(send_out, 0))
+            out_near(h)
+        out_far(0)
 
     def near_out(h):
         cid = near * parts + h
@@ -238,7 +251,7 @@
         @pl.when(inner)
         def _():
             relay_out(cid)
-            pl.when(h + 1 < parts)(lambda: both_ways(functools.partial(send_out, h + 1)))
+            pl.when(h + 1 < parts)(lambda: out_far(h + 1))
 
     for block in (block_l, block_f):
         for oy, ox in others:
@@ -269,8 +282,15 @@
 
     kept, given = core * half, (1 - core) * half
 
+    ready = [(k, h) for k in (1, 0) for h in range(parts)]
+    later = [(k, h) for k in range(2, n) for h in range(parts)]
+    later.sort(key=lambda v: (v[1] + FAR_STEP * (v[0] - 2), v[0]))
+
     def chunk(t):
-        k, h = t % n, t // n
+        code = jnp.int32(0)
+        for q, (k, h) in enumerate(ready + later):
+            code = jnp.where(t == q, k * parts + h, code)
+        k, h = code // parts, code % parts
         pair = lax.rem(i // PLANES + k // PLANES, n // PLANES)
         e = k % PLANES
         far = jnp.where(pair > i // PLANES, pair * PLANES + e, pair * PLANES + PLANES - 1 - e)
@@ -301,14 +321,13 @@
     def product(t):
         cid = chunk(t)
         cols = out_cols(cid)
-        k, h = t % n, t // n
-
-        @pl.when(k > 0)
+
+        @pl.when(cid // parts != near)
         def _():
             done(wo.at[:, cols], wo_recv.at[cid])
             relay_out(cid)
 
-        pl.when((k == 1) & (h + 1 < parts))(lambda: near_out(h + 1))
+        pl.when(t + 1 < parts)(lambda: near_out(t + 1))
 
         multiply(given, cols)
         remote(
@@ -386,7 +405,15 @@
         out[:, cols] = (f32(x_ref[:, cols]) + v).astype(jnp.bfloat16)
         pltpu.make_async_copy(out.at[:, cols], o_hbm.at[:, cols], o_sem).start()
 
-    stages = ((0, product), (LAG_1, first_stage), (LAG_2, second_stage), (LAG_3, third_stage), (LAG_4, finish))
+    def finish_far(t):
+        pl.when(t >= len(ready))(lambda: finish(t))
+
+    def finish_ready(t):
+        pl.when(t < len(ready))(lambda: finish(t))
+
+    LAG_5 = LAG_4 + parts
+    stages = ((0, product), (LAG_1, first_stage), (LAG_2, second_stage), (LAG_3, third_stage),
+              (LAG_4, finish_far), (LAG_5, finish_ready))
 
     @pl.loop(0, NC + LAG_4)
     def _(t):

time: 122 us -> 117 us (0.959)
  Pallas kernels: 119 us -> 114 us
    pallas_call x1, Pallas kernels: 119 us -> 114 us  [local(): pl.pallas_call(functools.partial(kernel, Y, n, X, parts), out_shape=jax.S...]
where the time goes in v2:
time: 117 us; the launch traced here: 116 us
  Pallas kernels  114 us (97%)
  local copies, waits for them, and re-layouts  1.88 us (2%)
    pallas_call x1, Pallas kernels, local(): pl.pallas_call(functools.partial(kernel, Y, n, X, parts), out_shape=jax.S...  114 us

profile of v2, /device:TPU:0, one launch (start us, length us, event | category | flops | bytes accessed | tf_op | source)
XLA Modules:
  0.0 116.4 jit_solution(17465205332791704347)
XLA Ops:
  0.0 114.5 %shard_map.46 = bf16[128,2048]{1,0:T(8,128)(2,1)} custom-call(bf16[128,2048]{1,0:T(8,128)(2,1)} %x_hbm.1, f32[1,2048]{1,0:T(1,128)} %bitcast.1, bf16[512,2048]{1,0:T(8,128)(2,1)} %wi_ref.1, bf16[2048,512]{1,0:T(8,128)(2,1)} %wo_ref.1), custom_call_target="tpu_custom_call" | custom-call | tf_op jit(solution)/shard_map/pallas_call | solution.py:464
  114.5 1.9 %copy.6 = bf16[128,2048]{1,0:T(8,128)(2,1)} copy(bf16[128,2048]{1,0:T(8,128)(2,1)} %shard_map.46) | data formatting | bytes 1048576

commit v3 on v2

--- a/solution.py
+++ b/solution.py
@@ -30,9 +30,9 @@
 
 
 def kernel(
-    Y, n, X, parts, x_hbm, g_ref, wi_ref, wo_ref, o_hbm,
-    norm, wi, wo, hid, crecv, yl, xf, xl, yf, own_l, own_f, zsend, zrecv, x_ref, out,
-    x_sem, o_sem, tok_send, tok_recv, wi_send, wi_recv, wo_send, wo_recv, wi_fwd, wo_fwd,
+    Y, n, X, parts, x_hbm, g_hbm, wi_ref, wo_ref, o_hbm,
+    norm, wi, wo, hid, crecv, yl, xf, xl, yf, own_l, own_f, zsend, zrecv, x_ref, g_ref, out,
+    x_sem, g_sem, o_sem, tok_send, tok_recv, wi_send, wi_recv, wo_send, wo_recv, wi_fwd, wo_fwd,
     c_send, c_recv, yl_send, yl_recv, xf_send, xf_recv, xl_send, xl_recv, yf_send, yf_recv, z_send, z_recv,
 ):
     y, i, j = lax.axis_index("grp"), lax.axis_index("fs"), lax.axis_index("tp")
@@ -69,6 +69,8 @@
 
     load_x = pltpu.make_async_copy(x_hbm, x_ref, x_sem)
     load_x.start()
+    load_g = pltpu.make_async_copy(g_hbm, g_ref, g_sem)
+    load_g.start()
 
     barrier = pltpu.get_barrier_semaphore()
     peers = len(others) + 1
@@ -117,6 +119,7 @@
         ).start()
 
     load_x.wait()
+    load_g.wait()
 
     @pl.loop(0, B // 16)
     def _(r):
@@ -459,12 +462,11 @@
         sends = 1 + 2 * chips + PLANES * (chips - 1)
         bf16 = jnp.bfloat16
         dma = pltpu.SemaphoreType.DMA
-        vmem = pl.BlockSpec(memory_space=pltpu.VMEM)
         hbm = pl.BlockSpec(memory_space=pl.ANY)
         return pl.pallas_call(
             functools.partial(kernel, Y, n, X, parts),
             out_shape=jax.ShapeDtypeStruct((B, D), bf16),
-            in_specs=[hbm, vmem, hbm, hbm],
+            in_specs=[hbm, hbm, hbm, hbm],
             out_specs=hbm,
             scratch_shapes=[
                 pltpu.VMEM((R, D), bf16),
@@ -481,8 +483,9 @@
                 pltpu.VMEM((B, D), bf16),
                 pltpu.VMEM((B, D), bf16),
                 pltpu.VMEM((B, D), bf16),
+                pltpu.VMEM((1, D), jnp.float32),
                 pltpu.VMEM((B, D), bf16),
-                dma, dma,
+                dma, dma, dma,
                 dma((sends,)), dma((CORES * chips * PLANES,)),
                 dma((4,)), dma((n,)),
                 dma((parts, 4)), dma((NC,)),

time: 117 us -> 116 us (level)
  no operation moved by 1% of the time
where the time goes in v3:
time: 116 us
  Pallas kernels  114 us (98%)
  local copies, waits for them, and re-layouts  1.88 us (2%)
    pallas_call x1, Pallas kernels, local(): pl.pallas_call(functools.partial(kernel, Y, n, X, parts), out_shape=jax.S...  114 us

profile of v3, /device:TPU:0, one launch (start us, length us, event | category | flops | bytes accessed | tf_op | source)
XLA Modules:
  0.0 115.7 jit_solution(10092102172874882108)
XLA Ops:
  0.0 113.8 %shard_map.46 = bf16[128,2048]{1,0:T(8,128)(2,1)} custom-call(bf16[128,2048]{1,0:T(8,128)(2,1)} %x_hbm.1, f32[1,2048]{1,0:T(1,128)} %bitcast.1, bf16[512,2048]{1,0:T(8,128)(2,1)} %wi_ref.1, bf16[2048,512]{1,0:T(8,128)(2,1)} %wo_ref.1), custom_call_target="tpu_custom_call" | custom-call | tf_op jit(solution)/shard_map/pallas_call | solution.py:466
  113.8 1.9 %copy.6 = bf16[128,2048]{1,0:T(8,128)(2,1)} copy(bf16[128,2048]{1,0:T(8,128)(2,1)} %shard_map.46) | data formatting | bytes 1048576

commit v4 on v3

--- a/solution.py
+++ b/solution.py
@@ -67,10 +67,6 @@
 
     HOPS = (1, 2, -1, -2)
 
-    load_x = pltpu.make_async_copy(x_hbm, x_ref, x_sem)
-    load_x.start()
-    load_g = pltpu.make_async_copy(g_hbm, g_ref, g_sem)
-    load_g.start()
 
     barrier = pltpu.get_barrier_semaphore()
     peers = len(others) + 1
@@ -87,6 +83,11 @@
         pl.semaphore_signal(
             barrier, inc=1, device_id=at(turn(y, oy, Y), turn(x, ox, X)), device_id_type=MESH
         )
+
+    load_x = pltpu.make_async_copy(x_hbm, x_ref, x_sem)
+    load_x.start()
+    load_g = pltpu.make_async_copy(g_hbm, g_ref, g_sem)
+    load_g.start()
 
     def block_l(c, yy, xx):
         return c * PLANES * chips + yy * X + xx

time: 116 us -> 116 us (level)
  no operation moved by 1% of the time
where the time goes in v4:
time: 116 us
  Pallas kernels  114 us (98%)
  local copies, waits for them, and re-layouts  1.88 us (2%)
    pallas_call x1, Pallas kernels, local(): pl.pallas_call(functools.partial(kernel, Y, n, X, parts), out_shape=jax.S...  114 us

profile of v4, /device:TPU:0, one launch (start us, length us, event | category | flops | bytes accessed | tf_op | source)
XLA Modules:
  0.0 115.9 jit_solution(12586536528086746135)
XLA Ops:
  0.0 114.0 %shard_map.46 = bf16[128,2048]{1,0:T(8,128)(2,1)} custom-call(bf16[128,2048]{1,0:T(8,128)(2,1)} %x_hbm.1, f32[1,2048]{1,0:T(1,128)} %bitcast.1, bf16[512,2048]{1,0:T(8,128)(2,1)} %wi_ref.1, bf16[2048,512]{1,0:T(8,128)(2,1)} %wo_ref.1), custom_call_target="tpu_custom_call" | custom-call | tf_op jit(solution)/shard_map/pallas_call | solution.py:467
  114.0 1.9 %copy.6 = bf16[128,2048]{1,0:T(8,128)(2,1)} copy(bf16[128,2048]{1,0:T(8,128)(2,1)} %shard_map.46) | data formatting | bytes 1048576
